TPU v7x, 32 devices: a whole 2x2x4 slice. The times are simulated.
32 devices in a mesh: kv: 8 (over z, x), tp: 4 (over y, core).
Axes of the slice: x: 2, y: 2, z: 4, core: 2. Of those that a mesh axis runs over, the one named last changes fastest.
Arguments:
- tokens: bfloat16 [1024, 2048], P('kv', 'tp'), may hold values from -6 to 6
- states: float32 [1024, 16, 64, 64], P('kv', 'tp'), may hold values from -6 to 6
- mix_gain: bfloat16 [2048], replicated, may hold values from 0.099609375 to 1.8984375
- w_query: bfloat16 [2048, 1024], P(None, 'tp'), may hold values from -0.125 to 0.125
- w_key: bfloat16 [2048, 1024], P(None, 'tp'), may hold values from -0.125 to 0.125
- w_value: bfloat16 [2048, 1024], P(None, 'tp'), may hold values from -0.125 to 0.125
- w_gate: bfloat16 [2048, 1024], P(None, 'tp'), may hold values from -0.125 to 0.125
- head_gain: bfloat16 [1024], P('tp'), may hold values from 0.099609375 to 1.8984375
- w_output: bfloat16 [1024, 2048], P('tp'), may hold values from -0.1875 to 0.1875
- channel_gain: bfloat16 [2048], replicated, may hold values from 0.099609375 to 1.8984375
- w_up: bfloat16 [2048, 8192], P(None, 'kv'), may hold values from -0.125 to 0.125
- w_down: bfloat16 [8192, 2048], P('kv'), may hold values from -0.0625 to 0.0625
Outputs:
- layer_out: bfloat16 [1024, 2048], P('kv', 'tp')
- new_states: float32 [1024, 16, 64, 64], P('kv', 'tp')
All inputs are finite; a program needn't handle non-finite values.
Results may differ from a plain program's by a relative error of at most 0.019.
Values may be sent and summed in bfloat16 or wider, within the bound.
A program may use at most 64 MiB of HBM per device.

v0:
```python
import jax
import jax.numpy as jnp
from jax import lax
from jax.sharding import PartitionSpec as P

HEADS = 16
POS = 16384


EPSILON = 1e-06
ROTARY_BASE = 10000.0


def rotate(vectors):
    half_size = vectors.shape[-1] // 2
    frequency = ROTARY_BASE ** (-jnp.arange(half_size, dtype=jnp.float32) / half_size)
    angles = POS * frequency
    cosine = jnp.cos(angles)
    sines = jnp.sin(angles)
    first_half = vectors[..., :half_size]
    second = vectors[..., half_size:]
    return jnp.concatenate(
        [first_half * cosine - second * sines, first_half * sines + second * cosine], axis=-1
    )


def retain(normed, states, w_query, w_key, w_value, w_gate, head_gain, head_ids):
    row_count = states.shape[0]
    head_count = states.shape[1]
    head_size = states.shape[2]

    def project(weight):
        return jnp.dot(normed, weight, preferred_element_type=jnp.float32).reshape(
            row_count, head_count, head_size
        )

    queries = rotate(project(w_query)) * head_size ** (-0.5)
    keys_now = rotate(project(w_key))
    values = project(w_value)
    gating = jnp.dot(normed, w_gate, preferred_element_type=jnp.float32)
    decays = 1.0 - jnp.exp2(-1.0 - 11.0 * head_ids / (HEADS - 1))
    new_states = (
        decays[None, :, None, None] * states + keys_now[:, :, :, None] * values[:, :, None, :]
    )
    output = jnp.einsum("bhk,bhkv->bhv", queries, new_states, precision=lax.Precision.HIGHEST)
    center = output - jnp.mean(output, axis=-1, keepdims=True)
    spread = jnp.mean(center * center, axis=-1, keepdims=True)
    scaled = (
        center
        * lax.rsqrt(spread + EPSILON)
        * head_gain.astype(jnp.float32).reshape(head_count, head_size)
    )
    gated_out = (scaled.reshape(row_count, head_count * head_size) * jax.nn.silu(gating)).astype(
        jnp.bfloat16
    )
    return (gated_out, new_states)


def activate(everyone, channel_gain, w_up):
    spread_rows = everyone.astype(jnp.float32)
    second_rms = lax.rsqrt(jnp.mean(spread_rows * spread_rows, axis=1, keepdims=True) + EPSILON)
    scaled = (spread_rows * channel_gain.astype(jnp.float32)).astype(jnp.bfloat16)
    hidden = jnp.dot(scaled, w_up, preferred_element_type=jnp.float32) * second_rms
    return jnp.square(jax.nn.relu(hidden)).astype(jnp.bfloat16)


def local(
    tokens,
    states,
    mix_gain,
    w_query,
    w_key,
    w_value,
    w_gate,
    head_gain,
    w_output,
    channel_gain,
    w_up,
    w_down,
):
    full_rows = lax.all_gather(tokens, "tp", axis=1, tiled=True)
    widened = full_rows.astype(jnp.float32)
    inverse_rms = lax.rsqrt(jnp.mean(widened * widened, axis=1, keepdims=True) + EPSILON)
    normed = (widened * inverse_rms * mix_gain.astype(jnp.float32)).astype(jnp.bfloat16)
    local_heads = states.shape[1]
    tp_index = lax.axis_index("tp")
    head_ids = (tp_index * local_heads + jnp.arange(local_heads)).astype(jnp.float32)
    gated_out, new_states = retain(
        normed, states, w_query, w_key, w_value, w_gate, head_gain, head_ids
    )
    partial_value = jnp.dot(gated_out, w_output, preferred_element_type=jnp.float32)
    attended = lax.psum_scatter(
        partial_value.astype(jnp.bfloat16), "tp", scatter_dimension=0, tiled=True
    ).astype(jnp.float32)
    share_rows = attended.shape[0]
    own_rows = lax.dynamic_slice_in_dim(full_rows, tp_index * share_rows, share_rows, 0)
    middle = (own_rows.astype(jnp.float32) + attended).astype(jnp.bfloat16)
    everyone = lax.all_gather(middle, "kv", axis=0, tiled=True)
    activated = activate(everyone, channel_gain, w_up)
    down_sum = lax.psum_scatter(
        jnp.dot(activated, w_down, preferred_element_type=jnp.float32).astype(jnp.bfloat16),
        "kv",
        scatter_dimension=0,
        tiled=True,
    ).astype(jnp.float32)
    finished = (middle.astype(jnp.float32) + down_sum).astype(jnp.bfloat16)
    layer_out = lax.all_to_all(finished, "tp", split_axis=1, concat_axis=0, tiled=True)
    return (layer_out, new_states)


def solution(mesh):
    placed = (
        P("kv", "tp"),
        P("kv", "tp", None, None),
        P(),
        P(None, "tp"),
        P(None, "tp"),
        P(None, "tp"),
        P(None, "tp"),
        P("tp"),
        P("tp", None),
        P(),
        P(None, "kv"),
        P("kv", None),
    )
    return jax.shard_map(
        local,
        mesh=mesh,
        in_specs=placed,
        out_specs=(P("kv", "tp"), P("kv", "tp", None, None)),
        check_vma=False,
    )
```

profile of v0, /device:TPU:0, one launch (start us, length us, event | category | flops | bytes accessed | tf_op | source)
XLA Modules:
  0.0 184.2 jit_solution(17715665310178965837)
XLA Ops:
  7.2 0.0 copy-start
  7.2 0.0 copy-start.3
  7.2 0.0 reduce-scatter.3.cloned.1.call-start
  7.3 0.1 fusion.15
  7.4 0.9 reshape.73
  8.3 0.7 convert_element_type.58
  9.0 8.9 %all_gather.6 = bf16[128,2048]{1,0:T(8,128)(2,1)S(1)} all-gather(bf16[128,512]{1,0:T(8,128)(2,1)} %param.12), channel_id=1, replica_groups=mesh['kv'=8,'tp'=4] {'tp'}, dimensions={1}, use_global_device_ids=true | all-gather | bytes 655360 | tf_op jit(solution)/shard_map/all_gather | solution.py:81
  17.9 0.2 fusion.5
  18.1 1.8 fusion.23
  19.9 1.8 fusion.21
  21.7 0.0 copy-done.3
  21.7 0.6 fusion.25
  22.3 0.1 multiply_subtract_fusion
  22.4 0.0 copy-start.4
  22.4 6.8 %multiply_reduce_fusion = (f32[128,4,64]{0,2,1:T(8,128)S(1)}, f32[128,4,64,64]{0,3,2,1:T(8,128)}) fusion(f32[128,4,64]{0,2,1:T(8,128)S(1)} %get-tuple-element.10, f32[128,4,64]{0,2,1:T(8,128)S(1)} %bitcast.22, f32[128,4,64]{0,2,1:T(8,128)S(1)} %get-tuple-element.11, f32[128,4,64,64]{0,3,2,1:T(8,128)} %param.13, f32[4]{0:T(128)S(1)} %exponential_subtract_fusion), kind=kLoop, calls=%fused_computation | loop fusion | flops 10452992 | bytes 17301520 | tf_op jit(solution)/shard_map/bhk,bhkv->bhv/dot_general | solution.py:45
  29.2 0.0 copy-start.2
  29.3 0.1 multiply_multiply_fusion
  29.4 0.1 copy.25
  29.5 0.0 copy-done
  29.5 0.0 copy-done.4
  29.5 1.6 convolution_convert_fusion.1
  31.2 0.0 reduce-scatter.3.cloned.1.call-update
  31.2 0.0 all-gather.2.cloned.1.call-start
  31.2 22.6 %reduce-scatter.3.cloned.1.call-done = bf16[32,2048]{1,0:T(8,128)(2,1)} async-done(((bf16[128,2048]{1,0:T(8,128)(2,1)}), bf16[32,2048]{1,0:T(8,128)(2,1)}) %reduce-scatter.3.cloned.1.call-update) | async-done | bytes 131088 | tf_op jit(solution)/shard_map/reduce_scatter | solution.py:92
  53.8 1.6 add_convert_fusion.1
  55.4 0.0 all-gather.2.cloned.1.call-update
  55.4 0.0 reduce-scatter.5.cloned.1.call-start
  55.5 0.0 copy-done.2
  55.5 41.3 %all-gather.2.cloned.1.call-done = bf16[256,2048]{1,0:T(8,128)(2,1)} async-done(((bf16[32,2048]{1,0:T(8,128)(2,1)}), bf16[256,2048]{1,0:T(8,128)(2,1)}) %all-gather.2.cloned.1.call-update) | async-done | bytes 1048592 | tf_op jit(solution)/shard_map/all_gather | solution.py:98
  96.8 1.5 fusion.1
  98.3 0.0 copy-start.1
  98.4 7.1 %convolution_convert_fusion = bf16[256,2048]{1,0:T(8,128)(2,1)} fusion(bf16[1024,2048]{1,0:T(8,128)(2,1)} %param.23, bf16[2048,1024]{1,0:T(8,128)(2,1)} %param.22, bf16[256,2048]{1,0:T(8,128)(2,1)} %all-gather.2.cloned.1.call-done, f32[2048]{0:T(1024)S(1)} %convert_element_type.67, f32[256]{0:T(256)S(1)} %add_rsqrt_fusion.1), kind=kOutput, calls=%fused_computation.4 | convolution fusion | flops 2150629376 | bytes 10494976 | tf_op jit(solution)/shard_map/dot_general | solution.py:101
  105.5 0.0 reduce-scatter.5.cloned.1.call-update
  105.5 63.4 %reduce-scatter.5.cloned.1.call-done = bf16[32,2048]{1,0:T(8,128)(2,1)} async-done(((bf16[256,2048]{1,0:T(8,128)(2,1)}), bf16[32,2048]{1,0:T(8,128)(2,1)}) %reduce-scatter.5.cloned.1.call-update) | async-done | bytes 131088 | tf_op jit(solution)/shard_map/reduce_scatter | solution.py:100
  168.9 0.0 copy-done.1
  168.9 0.9 add_convert_fusion
  169.9 7.1 %all_to_all.19 = bf16[32,4,512]{2,0,1:T(8,128)(2,1)S(1)} all-to-all(bf16[32,4,512]{2,0,1:T(8,128)(2,1)S(1)} %bitcast.21), channel_id=1, replica_groups=mesh['kv'=8,'tp'=4] {'tp'}, dimensions={1} | all-to-all | bytes 262144 | tf_op jit(solution)/shard_map/all_to_all | solution.py:107
  177.0 0.7 copy.40
  (11 shorter events, 0.2 us)
Async XLA Ops:
  7.2 22.4 %copy-start = (bf16[256,2048]{1,0:T(8,128)(2,1)S(1)}, bf16[256,2048]{1,0:T(8,128)(2,1)}, u32[]{:S(2)}) copy-start(bf16[256,2048]{1,0:T(8,128)(2,1)} %param.20) | copy-start | bytes 3145732
  7.2 14.5 %copy-start.3 = (bf16[2048,256]{1,0:T(8,128)(2,1)S(1)}, bf16[2048,256]{1,0:T(8,128)(2,1)}, u32[]{:S(2)}) copy-start(bf16[2048,256]{1,0:T(8,128)(2,1)} %param.15) | copy-start | bytes 3145732
  7.2 46.6 %reduce-scatter.3.cloned.1.call-start = ((), (), s32[]{:S(2)}) async-start(), calls=%async_computation.3 | async-start | bytes 655360 | tf_op jit(solution)/shard_map/reduce_scatter | solution.py:92
  22.4 7.1 %copy-start.4 = (bf16[2048,256]{1,0:T(8,128)(2,1)S(1)}, bf16[2048,256]{1,0:T(8,128)(2,1)}, u32[]{:S(2)}) copy-start(bf16[2048,256]{1,0:T(8,128)(2,1)} %param.18) | copy-start | bytes 3145732
  29.2 26.3 %copy-start.2 = (bf16[2048]{0:T(1024)(128)(2,1)S(1)}, bf16[2048]{0:T(1024)(128)(2,1)}, u32[]{:S(2)}) copy-start(bf16[2048]{0:T(1024)(128)(2,1)} %param.21) | copy-start | bytes 12292
  31.2 65.6 %all-gather.2.cloned.1.call-start = ((), (), s32[]{:S(2)}) async-start(), calls=%async_computation.4 | async-start | bytes 1179648 | tf_op jit(solution)/shard_map/all_gather | solution.py:98
  55.4 113.5 %reduce-scatter.5.cloned.1.call-start = ((), (), s32[]{:S(2)}) async-start(), calls=%async_computation.5 | async-start | bytes 1179648 | tf_op jit(solution)/shard_map/reduce_scatter | solution.py:100
  98.3 70.6 %copy-start.1 = (bf16[32,2048]{1,0:T(8,128)(2,1)S(1)}, bf16[32,2048]{1,0:T(8,128)(2,1)}, u32[]{:S(2)}) copy-start(bf16[32,2048]{1,0:T(8,128)(2,1)} %add_convert_fusion.1) | copy-start | bytes 393220
Sparse Core Ops, SparseCore 0:
  31.3 22.4 reduce-scatter.2
  56.5 40.2 all-gather.1
  105.6 63.2 reduce-scatter.4
where the time goes:
time: 185 us; the launch traced here: 184 us
  waiting for transfers between devices  127 us (69%)
  blocking collectives  16 us (9%)
  between operations  13.9 us (8%)
  matrix products  13 us (7%)
  other arithmetic  12.1 us (7%)
    reduce_scatter x1, waiting for transfers between devices, local(): lax.psum_scatter(jnp.dot(activated, w_down, preferred_element_type=jnp.fl...  63.4 us
    all_gather x1, waiting for transfers between devices, local(): everyone = lax.all_gather(middle, 'kv', axis=0, tiled=True)  41.3 us
    reduce_scatter x1, waiting for transfers between devices, local(): lax.psum_scatter(partial_value.astype(jnp.bfloat16), 'tp', scatter_dimens...  22.6 us
    all_gather x1, blocking collectives, local(): full_rows = lax.all_gather(tokens, 'tp', axis=1, tiled=True)  8.87 us
    all_to_all x1, blocking collectives, local(): lax.all_to_all(finished, 'tp', split_axis=1, concat_axis=0, tiled=True)  7.14 us
    dot_general x1, matrix products, local(): jnp.dot(activated, w_down, preferred_element_type=jnp.float32)  7.14 us
    dot_general x1, other arithmetic, retain(): jnp.einsum('bhk,bhkv->bhv', queries, new_states, precision=lax.Precision....  6.79 us
    dot_general x3, matrix products, project(): jnp.dot(normed, weight, preferred_element_type=jnp.float32)  4.19 us
  transfers between devices with their start and end apart: 3, of which 3 were waited for; matrix products, arithmetic and copies ran while one was open for 0% of the time, Pallas kernels for 0%

commit v1 on v0

v1 whole, which is shorter than its diff:
```python
import functools
import math

import jax
import jax.numpy as jnp
import numpy as np
from jax import lax
from jax.experimental import pallas as pl
from jax.experimental.pallas import tpu as pltpu
from jax.sharding import PartitionSpec as P

POS = 16384
EPSILON = 1e-06
ROTARY_BASE = 10000.0
CORES = 2
CHUNKS = 2
MESH = pl.DeviceIdType.MESH
F32 = jnp.float32
BF16 = jnp.bfloat16


def dot(a, b):
    return jnp.dot(a, b, preferred_element_type=F32)


def kernel(
    sizes,
    tok_hbm, st_hbm, mix_gain, wq_hbm, wk_hbm, wv_hbm, wg_hbm, head_gain, wo_hbm,
    chan_gain, wu_hbm, wd_hbm, turn,
    out_ref, new_hbm,
    xf, wproj, st, wo, wu, wd, acc, qt, kt, vt, rt,
    part, r1, s2, r2, mid, lhs, act, sx, rx, sz, rz, fin, ob,
    load_sem, store_sem, a_send, a_recv, b1_send, b1_recv, b2_send, b2_recv,
    cz_send, cx_send, c_recv, dx_send, dx_recv, dz_send, dz_recv, e_send, e_recv,
):
    n_tp, ny, nz, nx, heads, head, rows, feats, share, width = sizes
    tp = lax.axis_index("tp")
    kv = lax.axis_index("kv")
    c, y = lax.rem(tp, CORES), tp // CORES
    x, z = lax.rem(kv, nx), kv // nx
    other = 1 - c
    partner = y * CORES + other
    half = head // 2
    piece = width // CHUNKS
    sent = []

    def ys(d):
        return lax.rem(y + d, ny)

    def zs(d):
        return lax.rem(z + d, nz)

    def xs(d):
        return lax.rem(x + d, nx)

    def make(src, dst, ssem, rsem, device):
        return pltpu.make_async_remote_copy(
            src_ref=src, dst_ref=dst, send_sem=ssem, recv_sem=rsem,
            device_id=device, device_id_type=MESH,
        )

    def send(src, dst, ssem, rsem, device):
        copy = make(src, dst, ssem, rsem, device)
        copy.start()
        sent.append(copy)

    def arrive(dst, ssem, rsem, device):
        make(dst, dst, ssem, rsem, device).wait_recv()

    barrier = pltpu.get_barrier_semaphore()
    greeted = 0
    for d in range(1, n_tp):
        pl.semaphore_signal(barrier, inc=1, device_id={"tp": lax.rem(tp + d, n_tp)}, device_id_type=MESH)
        greeted += 1
    for d in range(1, nx):
        pl.semaphore_signal(barrier, inc=1, device_id={"kv": z * nx + xs(d)}, device_id_type=MESH)
        greeted += 1
    for d in range(1, nz):
        pl.semaphore_signal(barrier, inc=1, device_id={"kv": zs(d) * nx + x}, device_id_type=MESH)
        greeted += 1

    loads = [pltpu.make_async_copy(tok_hbm, xf.at[tp], load_sem.at[0])]
    for i, w in enumerate((wq_hbm, wk_hbm, wv_hbm, wg_hbm)):
        loads.append(pltpu.make_async_copy(w, wproj.at[i], load_sem.at[1 + i]))
    for h in range(heads):
        loads.append(pltpu.make_async_copy(st_hbm.at[h], st.at[h], load_sem.at[5 + h]))
    loads.append(pltpu.make_async_copy(wo_hbm, wo, load_sem.at[5 + heads]))
    loads.append(pltpu.make_async_copy(wu_hbm, wu, load_sem.at[6 + heads]))
    loads.append(pltpu.make_async_copy(wd_hbm, wd, load_sem.at[7 + heads]))
    for copy in loads:
        copy.start()
    loads[0].wait()
    pl.semaphore_wait(barrier, greeted)

    for d in range(1, ny):
        send(xf.at[tp], xf.at[tp], a_send.at[d], a_recv.at[tp], {"tp": ys(d) * CORES + c})
    send(xf.at[tp], xf.at[tp], a_send.at[0], a_recv.at[tp], {"tp": partner})

    squares = jnp.zeros((rows, 1), F32)

    def project(slot, first, squares):
        at = pl.ds(pl.multiple_of(slot * feats, feats), feats)
        wide = xf[slot].astype(F32)
        scaled = (wide * mix_gain[:, at].astype(F32)).astype(BF16)
        for i in range(4):
            if first:
                loads[1 + i].wait()
            term = dot(scaled, wproj[i, at, :])
            if first:
                acc[i] = term
            else:
                acc[i] += term
        return squares + jnp.sum(wide * wide, axis=1, keepdims=True)

    squares = project(tp, True, squares)
    arrive(xf.at[partner], a_send.at[0], a_recv.at[partner], {"tp": partner})
    squares = project(partner, False, squares)
    for d in range(1, ny):
        slot = ys(d) * CORES + c
        arrive(xf.at[slot], a_send.at[0], a_recv.at[slot], {"tp": slot})
        send(xf.at[slot], xf.at[slot], a_send.at[ny + d], a_recv.at[slot], {"tp": partner})
        squares = project(slot, False, squares)
        slot = ys(d) * CORES + other
        arrive(xf.at[slot], a_send.at[0], a_recv.at[slot], {"tp": partner})
        squares = project(slot, False, squares)
    inverse = lax.rsqrt(squares * (1.0 / width) + EPSILON)

    qt[...] = (acc[0] * inverse).T
    kt[...] = (acc[1] * inverse).T
    vt[...] = (acc[2] * inverse).T
    cosine, sine = turn[:half, :], turn[half:, :]
    for h in range(heads):
        lo, hi = pl.ds(h * head, half), pl.ds(h * head + half, half)
        for ref, scale in ((qt, head ** -0.5), (kt, 1.0)):
            a, b = ref[lo, :], ref[hi, :]
            ref[lo, :] = (a * cosine - b * sine) * scale
            ref[hi, :] = (a * sine + b * cosine) * scale
    stores = []
    for h in range(heads):
        loads[5 + h].wait()
        number = (tp * heads + h).astype(F32)
        decay = 1.0 - jnp.exp2(-1.0 - 11.0 * jnp.full((1, rows), number, F32) / (heads * n_tp - 1))
        value = vt[pl.ds(h * head, head), :]
        base = h * head

        def step(k, total, h=h, base=base, decay=decay, value=value):
            fresh = decay * st[h, k] + kt[pl.ds(base + k, 1), :] * value
            st[h, k] = fresh
            return total + qt[pl.ds(base + k, 1), :] * fresh

        total = lax.fori_loop(0, head, step, jnp.zeros((head, rows), F32), unroll=8)
        center = total - jnp.mean(total, axis=0, keepdims=True)
        spread = jnp.mean(center * center, axis=0, keepdims=True)
        rt[pl.ds(base, head), :] = center * lax.rsqrt(spread + EPSILON)
        copy = pltpu.make_async_copy(st.at[h], new_hbm.at[h], store_sem.at[h])
        copy.start()
        stores.append(copy)
    gating = acc[3] * inverse
    gated = (rt[...].T * head_gain[...].astype(F32) * (gating * jax.nn.sigmoid(gating))).astype(BF16)

    loads[5 + heads].wait()
    for j in range(CHUNKS):
        whole = dot(gated, wo[:, j * piece:(j + 1) * piece]).astype(BF16)
        for t in range(n_tp):
            part[j, t] = whole[t * share:(t + 1) * share]
        for d in range(ny):
            to = ys(d)
            send(part.at[j, to * CORES + other], r1.at[j, to], b1_send.at[j, d], b1_recv.at[j, to], {"tp": partner})

    def pair_sum(j, to):
        arrive(r1.at[j, to], b1_send.at[0, 0], b1_recv.at[j, to], {"tp": partner})
        return part[j, to * CORES + c].astype(F32) + r1[j, to].astype(F32)

    for j in range(CHUNKS):
        for d in range(1, ny):
            to = ys(d)
            s2[j, to] = pair_sum(j, to).astype(BF16)
            send(s2.at[j, to], r2.at[j, y], b2_send.at[j, d], b2_recv.at[j, y], {"tp": to * CORES + c})
    own_rows = pl.ds(pl.multiple_of(tp * share, share), share)
    for j in range(CHUNKS):
        total = pair_sum(j, y)
        for d in range(1, ny):
            frm = ys(d)
            arrive(r2.at[j, frm], b2_send.at[0, 0], b2_recv.at[j, frm], {"tp": frm * CORES + c})
            total += r2[j, frm].astype(F32)
        per = n_tp // CHUNKS
        mine = jnp.concatenate([xf[t, own_rows, :] for t in range(j * per, (j + 1) * per)], axis=1)
        mid[z, x, j] = (mine.astype(F32) + total).astype(BF16)
        for d in range(1, nz):
            send(mid.at[z, x, j], mid.at[z, x, j], cz_send.at[j, d], c_recv.at[z, x, j], {"kv": zs(d) * nx + x})
        for d in range(1, nx):
            send(mid.at[z, x, j], mid.at[z, x, j], cx_send.at[j, 0, d], c_recv.at[z, x, j], {"kv": z * nx + xs(d)})

    def forward(e):
        for j in range(CHUNKS):
            zz = zs(e)
            arrive(mid.at[zz, x, j], cz_send.at[0, 0], c_recv.at[zz, x, j], {"kv": zz * nx + x})
            for d in range(1, nx):
                send(mid.at[zz, x, j], mid.at[zz, x, j], cx_send.at[j, e, d], c_recv.at[zz, x, j], {"kv": z * nx + xs(d)})

    tall = nx * share
    hidden_units = wu.shape[1]
    up_tile = min(256, hidden_units)
    down_tile = 256

    def mixer(e):
        zz = zs(e)
        for d in range(1, nx):
            for j in range(CHUNKS):
                xx = xs(d)
                arrive(mid.at[zz, xx, j], cz_send.at[0, 0], c_recv.at[zz, xx, j], {"kv": z * nx + xx})
        sums = jnp.zeros((tall, 1), F32)
        for j in range(CHUNKS):
            wide = mid[zz, :, j].reshape(tall, piece).astype(F32)
            sums += jnp.sum(wide * wide, axis=1, keepdims=True)
            lhs[:, j * piece:(j + 1) * piece] = (
                wide * chan_gain[:, j * piece:(j + 1) * piece].astype(F32)
            ).astype(BF16)
        rms = lax.rsqrt(sums * (1.0 / width) + EPSILON)
        if e == 0:
            loads[6 + heads].wait()

        @pl.loop(0, hidden_units // up_tile)
        def _(i):
            at = pl.ds(pl.multiple_of(i * up_tile, up_tile), up_tile)
            hidden = jnp.maximum(dot(lhs[...], wu[:, at]) * rms, 0.0)
            act[:, at] = (hidden * hidden).astype(BF16)

        if e == 0:
            loads[7 + heads].wait()

        @pl.loop(0, width // down_tile)
        def _(i):
            at = pl.ds(pl.multiple_of(i * down_tile, down_tile), down_tile)
            down = dot(act[...], wd[:, at])
            for xx in range(nx):
                sx[e, xx, :, at] = down[xx * share:(xx + 1) * share].astype(BF16)

        for d in range(1, nx):
            xx = xs(d)
            send(sx.at[e, xx], rx.at[e, x], dx_send.at[e, d], dx_recv.at[e, x], {"kv": z * nx + xx})

    def reduce_x(e):
        total = sx[e, x].astype(F32)
        for d in range(1, nx):
            xx = xs(d)
            arrive(rx.at[e, xx], dx_send.at[0, 0], dx_recv.at[e, xx], {"kv": z * nx + xx})
            total += rx[e, xx].astype(F32)
        return total

    def reduce_z(e):
        sz[e] = reduce_x(e).astype(BF16)
        send(sz.at[e], rz.at[z], dz_send.at[e], dz_recv.at[z], {"kv": zs(e) * nx + x})

    for e in range(nz):
        if e + 1 < nz:
            forward(e + 1)
        mixer(e)
        if e >= 2:
            reduce_z(e - 1)
    if nz > 1:
        reduce_z(nz - 1)
    total = reduce_x(0)
    total += jnp.concatenate([mid[z, x, j] for j in range(CHUNKS)], axis=1).astype(F32)
    for d in range(1, nz):
        zz = zs(d)
        arrive(rz.at[zz], dz_send.at[0], dz_recv.at[zz], {"kv": zz * nx + x})
        total += rz[zz].astype(F32)
    done = total.astype(BF16)
    for t in range(n_tp):
        fin[t] = done[:, t * feats:(t + 1) * feats]
    for d in range(1, n_tp):
        to = lax.rem(tp + d, n_tp)
        send(fin.at[to], ob.at[tp], e_send.at[d], e_recv.at[tp], {"tp": to})
    ob[tp] = fin[tp]
    for d in range(1, n_tp):
        frm = lax.rem(tp + d, n_tp)
        arrive(ob.at[frm], e_send.at[0], e_recv.at[frm], {"tp": frm})
    out_ref[...] = ob[...].reshape(rows, feats)
    for copy in sent:
        copy.wait_send()
    for copy in stores:
        copy.wait()


def local(
    n_kv, n_tp,
    tokens, states, mix_gain, w_query, w_key, w_value, w_gate, head_gain, w_output,
    channel_gain, w_up, w_down,
):
    rows, feats = tokens.shape
    heads, head = states.shape[1], states.shape[2]
    width = mix_gain.shape[0]
    inner = w_query.shape[1]
    hidden = w_up.shape[1]
    share = rows // n_tp
    nx = 1
    while (2 * nx) ** 2 <= n_kv:
        nx *= 2
    nz = n_kv // nx
    ny = n_tp // CORES
    piece = width // CHUNKS
    angles = POS * ROTARY_BASE ** (-np.arange(head // 2) / (head // 2))
    turn = np.concatenate([np.cos(angles), np.sin(angles)])[:, None]
    turn = jnp.asarray(np.broadcast_to(turn, (head, rows)), F32)
    sizes = (n_tp, ny, nz, nx, heads, head, rows, feats, share, width)
    hbm = pl.BlockSpec(memory_space=pl.ANY)
    vmem = pl.BlockSpec(memory_space=pltpu.VMEM)
    dma = pltpu.SemaphoreType.DMA
    layer_out, new_states = pl.pallas_call(
        functools.partial(kernel, sizes),
        out_shape=(
            jax.ShapeDtypeStruct((rows, feats), BF16),
            jax.ShapeDtypeStruct((heads, head, head, rows), F32),
        ),
        in_specs=[hbm, hbm, vmem, hbm, hbm, hbm, hbm, vmem, hbm, vmem, hbm, hbm, vmem],
        out_specs=(vmem, hbm),
        scratch_shapes=[
            pltpu.VMEM((n_tp, rows, feats), BF16),
            pltpu.VMEM((4, width, inner), BF16),
            pltpu.VMEM((heads, head, head, rows), F32),
            pltpu.VMEM((inner, width), BF16),
            pltpu.VMEM((width, hidden), BF16),
            pltpu.VMEM((hidden, width), BF16),
            pltpu.VMEM((4, rows, inner), F32),
            pltpu.VMEM((inner, rows), F32),
            pltpu.VMEM((inner, rows), F32),
            pltpu.VMEM((inner, rows), F32),
            pltpu.VMEM((inner, rows), F32),
            pltpu.VMEM((CHUNKS, n_tp, share, piece), BF16),
            pltpu.VMEM((CHUNKS, ny, share, piece), BF16),
            pltpu.VMEM((CHUNKS, ny, share, piece), BF16),
            pltpu.VMEM((CHUNKS, ny, share, piece), BF16),
            pltpu.VMEM((nz, nx, CHUNKS, share, piece), BF16),
            pltpu.VMEM((nx * share, width), BF16),
            pltpu.VMEM((nx * share, hidden), BF16),
            pltpu.VMEM((nz, nx, share, width), BF16),
            pltpu.VMEM((nz, nx, share, width), BF16),
            pltpu.VMEM((nz, share, width), BF16),
            pltpu.VMEM((nz, share, width), BF16),
            pltpu.VMEM((n_tp, share, feats), BF16),
            pltpu.VMEM((n_tp, share, feats), BF16),
            dma((8 + heads,)),
            dma((heads,)),
            dma((2 * ny,)),
            dma((n_tp,)),
            dma((CHUNKS, ny)),
            dma((CHUNKS, ny)),
            dma((CHUNKS, ny)),
            dma((CHUNKS, ny)),
            dma((CHUNKS, nz)),
            dma((CHUNKS, nz, nx)),
            dma((nz, nx, CHUNKS)),
            dma((nz, nx)),
            dma((nz, nx)),
            dma((nz,)),
            dma((nz,)),
            dma((n_tp,)),
            dma((n_tp,)),
        ],
        compiler_params=pltpu.CompilerParams(
            collective_id=0, has_side_effects=True, vmem_limit_bytes=56 * 1024 * 1024
        ),
    )(
        tokens, jnp.transpose(states, (1, 2, 3, 0)), mix_gain[None], w_query, w_key, w_value,
        w_gate, head_gain[None], w_output, channel_gain[None], w_up, w_down, turn,
    )
    return (layer_out, jnp.transpose(new_states, (3, 0, 1, 2)))


def solution(mesh):
    placed = (
        P("kv", "tp"),
        P("kv", "tp", None, None),
        P(),
        P(None, "tp"),
        P(None, "tp"),
        P(None, "tp"),
        P(None, "tp"),
        P("tp"),
        P("tp", None),
        P(),
        P(None, "kv"),
        P("kv", None),
    )
    return jax.shard_map(
        functools.partial(local, mesh.shape["kv"], mesh.shape["tp"]),
        mesh=mesh,
        in_specs=placed,
        out_specs=(P("kv", "tp"), P("kv", "tp", None, None)),
        check_vma=False,
    )
```

time: 185 us -> 76.4 us (0.41)
  waiting for transfers between devices: 127 us -> 0 us
  Pallas kernels: 0 us -> 61.6 us
  blocking collectives: 16 us -> 0 us
  between operations: 13.9 us -> 0.64 us
  matrix products: 13 us -> 0 us
  other arithmetic: 12.1 us -> 0 us
  local copies, waits for them, and re-layouts: 1.71 us -> 13.8 us
    reduce_scatter x2 -> x0, waiting for transfers between devices: 86 us -> none  [the longest x1 63.4 us: local(): lax.psum_scatter(jnp.dot(activated, w_down, preferred_element_type=jnp.fl...]
    pallas_call x0 -> x1, Pallas kernels: none -> 61.6 us  [local(): pl.pallas_call(functools.partial(kernel, sizes), out_shape=(jax.ShapeDtyp...]
    all_gather x1 -> x0, waiting for transfers between devices: 41.3 us -> none  [local(): everyone = lax.all_gather(middle, 'kv', axis=0, tiled=True)]
    dot_general x5 -> x0, matrix products: 13 us -> none  [the longest x1 7.14 us: local(): jnp.dot(activated, w_down, preferred_element_type=jnp.float32)]
    unnamed x11 -> x2, local copies, waits for them, and re-layouts: 0.69 us -> 10 us
    all_gather x1 -> x0, blocking collectives: 8.87 us -> none  [local(): full_rows = lax.all_gather(tokens, 'tp', axis=1, tiled=True)]
    all_to_all x1 -> x0, blocking collectives: 7.14 us -> none  [local(): lax.all_to_all(finished, 'tp', split_axis=1, concat_axis=0, tiled=True)]
    dot_general x1 -> x0, other arithmetic: 6.79 us -> none  [retain(): jnp.einsum('bhk,bhkv->bhv', queries, new_states, precision=lax.Precision....]
  transfers between devices with their start and end apart: 3 -> 0, of which waited for: 3 -> 0; matrix products, arithmetic and copies ran while one was open for 0% -> 0% of each run, Pallas kernels for 0% -> 0%
where the time goes in v1:
time: 76.4 us; the launch traced here: 76.1 us
  Pallas kernels  61.6 us (81%)
  local copies, waits for them, and re-layouts  13.8 us (18%)
    pallas_call x1, Pallas kernels, local(): pl.pallas_call(functools.partial(kernel, sizes), out_shape=(jax.ShapeDtyp...  61.6 us
    unnamed x2, local copies, waits for them, and re-layouts  10 us

profile of v1, /device:TPU:0, one launch (start us, length us, event | category | flops | bytes accessed | tf_op | source)
XLA Modules:
  0.0 76.1 jit_solution(5374946502890468264)
XLA Ops:
  0.6 1.2 %broadcast_in_dim.10.head_gain = bf16[1,256]{1,0:T(2,128)(2,1)} reshape(bf16[256]{0:T(256)(128)(2,1)} %param.20) | data formatting | bytes 1024 | tf_op jit(solution)/shard_map/broadcast_in_dim | solution.py:366
  1.9 1.3 %broadcast_in_dim.9.mix_gain = bf16[1,2048]{1,0:T(2,128)(2,1)} reshape(bf16[2048]{0:T(1024)(128)(2,1)} %param.15) | data formatting | bytes 8192 | tf_op jit(solution)/shard_map/broadcast_in_dim | solution.py:365
  3.2 1.3 %broadcast_in_dim.11.chan_gain = bf16[1,2048]{1,0:T(2,128)(2,1)} reshape(bf16[2048]{0:T(1024)(128)(2,1)} %param.22) | data formatting | bytes 8192 | tf_op jit(solution)/shard_map/broadcast_in_dim | solution.py:366
  4.4 61.6 %shard_map.140 = (bf16[128,512]{1,0:T(8,128)(2,1)}, f32[4,64,64,128]{3,2,1,0:T(8,128)}) custom-call(bf16[128,512]{1,0:T(8,128)(2,1)} %tok_hbm.1, f32[4,64,64,128]{3,2,1,0:T(8,128)} %bitcast.2, bf16[1,2048]{1,0:T(2,128)(2,1)} %broadcast_in_dim.9.mix_gain, bf16[2048,256]{1,0:T(8,128)(2,1)} %wq_hbm.1, bf16[2048,256]{1,0:T(8,128)(2,1)} %wk_hbm.1, ...), custom_call_target="tpu_custom_call" | custom-call | tf_op jit(solution)/shard_map/pallas_call | solution.py:310
  66.1 1.6 %copy.17 = bf16[128,512]{1,0:T(8,128)(2,1)} copy(bf16[128,512]{1,0:T(8,128)(2,1)} %get-tuple-element.8) | data formatting | bytes 262144
  67.6 8.4 %copy.18 = f32[128,4,64,64]{0,3,2,1:T(8,128)} copy(f32[128,4,64,64]{0,3,2,1:T(8,128)} %bitcast.3) | data formatting | bytes 16777216

commit v2 on v1

--- a/solution.py
+++ b/solution.py
@@ -14,6 +14,7 @@
 ROTARY_BASE = 10000.0
 CORES = 2
 CHUNKS = 2
+SLICES = 4
 MESH = pl.DeviceIdType.MESH
 F32 = jnp.float32
 BF16 = jnp.bfloat16
@@ -27,10 +28,10 @@
     sizes,
     tok_hbm, st_hbm, mix_gain, wq_hbm, wk_hbm, wv_hbm, wg_hbm, head_gain, wo_hbm,
     chan_gain, wu_hbm, wd_hbm, turn,
-    out_ref, new_hbm,
-    xf, wproj, st, wo, wu, wd, acc, qt, kt, vt, rt,
+    out_ref, st,
+    gain1, gain2, xf, wproj, wo, wu, wd, acc, qt, kt, vt, rt,
     part, r1, s2, r2, mid, lhs, act, sx, rx, sz, rz, fin, ob,
-    load_sem, store_sem, a_send, a_recv, b1_send, b1_recv, b2_send, b2_recv,
+    load_sem, a_send, a_recv, b1_send, b1_recv, b2_send, b2_recv,
     cz_send, cx_send, c_recv, dx_send, dx_recv, dz_send, dz_recv, e_send, e_recv,
 ):
     n_tp, ny, nz, nx, heads, head, rows, feats, share, width = sizes
@@ -42,6 +43,7 @@
     partner = y * CORES + other
     half = head // 2
     piece = width // CHUNKS
+    strip = width // SLICES
     sent = []
 
     def ys(d):
@@ -89,6 +91,8 @@
     loads.append(pltpu.make_async_copy(wd_hbm, wd, load_sem.at[7 + heads]))
     for copy in loads:
         copy.start()
+    gain1[...] = mix_gain[...].astype(F32).reshape(1, width)
+    gain2[...] = chan_gain[...].astype(F32).reshape(1, width)
     loads[0].wait()
     pl.semaphore_wait(barrier, greeted)
 
@@ -101,7 +105,7 @@
     def project(slot, first, squares):
         at = pl.ds(pl.multiple_of(slot * feats, feats), feats)
         wide = xf[slot].astype(F32)
-        scaled = (wide * mix_gain[:, at].astype(F32)).astype(BF16)
+        scaled = (wide * gain1[:, at]).astype(BF16)
         for i in range(4):
             if first:
                 loads[1 + i].wait()
@@ -135,7 +139,6 @@
             a, b = ref[lo, :], ref[hi, :]
             ref[lo, :] = (a * cosine - b * sine) * scale
             ref[hi, :] = (a * sine + b * cosine) * scale
-    stores = []
     for h in range(heads):
         loads[5 + h].wait()
         number = (tp * heads + h).astype(F32)
@@ -152,11 +155,8 @@
         center = total - jnp.mean(total, axis=0, keepdims=True)
         spread = jnp.mean(center * center, axis=0, keepdims=True)
         rt[pl.ds(base, head), :] = center * lax.rsqrt(spread + EPSILON)
-        copy = pltpu.make_async_copy(st.at[h], new_hbm.at[h], store_sem.at[h])
-        copy.start()
-        stores.append(copy)
     gating = acc[3] * inverse
-    gated = (rt[...].T * head_gain[...].astype(F32) * (gating * jax.nn.sigmoid(gating))).astype(BF16)
+    gated = (rt[...].T * head_gain[...].astype(F32).reshape(1, heads * head) * (gating * jax.nn.sigmoid(gating))).astype(BF16)
 
     loads[5 + heads].wait()
     for j in range(CHUNKS):
@@ -214,7 +214,7 @@
             wide = mid[zz, :, j].reshape(tall, piece).astype(F32)
             sums += jnp.sum(wide * wide, axis=1, keepdims=True)
             lhs[:, j * piece:(j + 1) * piece] = (
-                wide * chan_gain[:, j * piece:(j + 1) * piece].astype(F32)
+                wide * gain2[:, j * piece:(j + 1) * piece]
             ).astype(BF16)
         rms = lax.rsqrt(sums * (1.0 / width) + EPSILON)
         if e == 0:
@@ -229,28 +229,29 @@
         if e == 0:
             loads[7 + heads].wait()
 
-        @pl.loop(0, width // down_tile)
-        def _(i):
-            at = pl.ds(pl.multiple_of(i * down_tile, down_tile), down_tile)
-            down = dot(act[...], wd[:, at])
-            for xx in range(nx):
-                sx[e, xx, :, at] = down[xx * share:(xx + 1) * share].astype(BF16)
-
+        for q in range(SLICES):
+            for i in range(strip // down_tile):
+                down = dot(act[...], wd[:, q * strip + i * down_tile:q * strip + (i + 1) * down_tile])
+                for xx in range(nx):
+                    sx[e, xx, q, :, i * down_tile:(i + 1) * down_tile] = (
+                        down[xx * share:(xx + 1) * share].astype(BF16)
+                    )
+            for d in range(1, nx):
+                xx = xs(d)
+                send(sx.at[e, xx, q], rx.at[e, x, q], dx_send.at[e, d, q], dx_recv.at[e, x, q], {"kv": z * nx + xx})
+
+    def reduce_x(e, q):
+        total = sx[e, x, q].astype(F32)
         for d in range(1, nx):
             xx = xs(d)
-            send(sx.at[e, xx], rx.at[e, x], dx_send.at[e, d], dx_recv.at[e, x], {"kv": z * nx + xx})
-
-    def reduce_x(e):
-        total = sx[e, x].astype(F32)
-        for d in range(1, nx):
-            xx = xs(d)
-            arrive(rx.at[e, xx], dx_send.at[0, 0], dx_recv.at[e, xx], {"kv": z * nx + xx})
-            total += rx[e, xx].astype(F32)
+            arrive(rx.at[e, xx, q], dx_send.at[0, 0, 0], dx_recv.at[e, xx, q], {"kv": z * nx + xx})
+            total += rx[e, xx, q].astype(F32)
         return total
 
     def reduce_z(e):
-        sz[e] = reduce_x(e).astype(BF16)
-        send(sz.at[e], rz.at[z], dz_send.at[e], dz_recv.at[z], {"kv": zs(e) * nx + x})
+        for q in range(SLICES):
+            sz[e, q] = reduce_x(e, q).astype(BF16)
+            send(sz.at[e, q], rz.at[z, q], dz_send.at[e, q], dz_recv.at[z, q], {"kv": zs(e) * nx + x})
 
     for e in range(nz):
         if e + 1 < nz:
@@ -260,27 +261,35 @@
             reduce_z(e - 1)
     if nz > 1:
         reduce_z(nz - 1)
-    total = reduce_x(0)
-    total += jnp.concatenate([mid[z, x, j] for j in range(CHUNKS)], axis=1).astype(F32)
-    for d in range(1, nz):
-        zz = zs(d)
-        arrive(rz.at[zz], dz_send.at[0], dz_recv.at[zz], {"kv": zz * nx + x})
-        total += rz[zz].astype(F32)
-    done = total.astype(BF16)
-    for t in range(n_tp):
-        fin[t] = done[:, t * feats:(t + 1) * feats]
-    for d in range(1, n_tp):
-        to = lax.rem(tp + d, n_tp)
-        send(fin.at[to], ob.at[tp], e_send.at[d], e_recv.at[tp], {"tp": to})
-    ob[tp] = fin[tp]
+    per_piece, per_strip = piece // strip, strip // feats
+    for q in range(SLICES):
+        inside = q % per_piece
+        total = reduce_x(0, q)
+        total += mid[z, x, q // per_piece, :, inside * strip:(inside + 1) * strip].astype(F32)
+        for d in range(1, nz):
+            zz = zs(d)
+            arrive(rz.at[zz, q], dz_send.at[0, 0], dz_recv.at[zz, q], {"kv": zz * nx + x})
+            total += rz[zz, q].astype(F32)
+        done = total.astype(BF16)
+        for i in range(per_strip):
+            t = q * per_strip + i
+            fin[t] = done[:, i * feats:(i + 1) * feats]
+
+            @pl.when(tp != t)
+            def _(t=t):
+                make(fin.at[t], ob.at[tp], e_send.at[t], e_recv.at[tp], {"tp": t}).start()
+
+            @pl.when(tp == t)
+            def _(t=t):
+                ob[tp] = fin[t]
+
     for d in range(1, n_tp):
         frm = lax.rem(tp + d, n_tp)
         arrive(ob.at[frm], e_send.at[0], e_recv.at[frm], {"tp": frm})
+        make(fin.at[frm], ob.at[tp], e_send.at[frm], e_recv.at[tp], {"tp": frm}).wait_send()
     out_ref[...] = ob[...].reshape(rows, feats)
     for copy in sent:
         copy.wait_send()
-    for copy in stores:
-        copy.wait()
 
 
 def local(
@@ -300,25 +309,27 @@
     nz = n_kv // nx
     ny = n_tp // CORES
     piece = width // CHUNKS
+    strip = width // SLICES
     angles = POS * ROTARY_BASE ** (-np.arange(head // 2) / (head // 2))
     turn = np.concatenate([np.cos(angles), np.sin(angles)])[:, None]
     turn = jnp.asarray(np.broadcast_to(turn, (head, rows)), F32)
     sizes = (n_tp, ny, nz, nx, heads, head, rows, feats, share, width)
-    hbm = pl.BlockSpec(memory_space=pl.ANY)
+    hbm = pl.BlockSpec(memory_space=pltpu.HBM)
     vmem = pl.BlockSpec(memory_space=pltpu.VMEM)
     dma = pltpu.SemaphoreType.DMA
     layer_out, new_states = pl.pallas_call(
         functools.partial(kernel, sizes),
         out_shape=(
-            jax.ShapeDtypeStruct((rows, feats), BF16),
-            jax.ShapeDtypeStruct((heads, head, head, rows), F32),
+            pltpu.VMEM((rows, feats), BF16),
+            pltpu.VMEM((heads, head, head, rows), F32),
         ),
         in_specs=[hbm, hbm, vmem, hbm, hbm, hbm, hbm, vmem, hbm, vmem, hbm, hbm, vmem],
-        out_specs=(vmem, hbm),
+        out_specs=(vmem, vmem),
         scratch_shapes=[
+            pltpu.VMEM((1, width), F32),
+            pltpu.VMEM((1, width), F32),
             pltpu.VMEM((n_tp, rows, feats), BF16),
             pltpu.VMEM((4, width, inner), BF16),
-            pltpu.VMEM((heads, head, head, rows), F32),
             pltpu.VMEM((inner, width), BF16),
             pltpu.VMEM((width, hidden), BF16),
             pltpu.VMEM((hidden, width), BF16),
@@ -334,14 +345,13 @@
             pltpu.VMEM((nz, nx, CHUNKS, share, piece), BF16),
             pltpu.VMEM((nx * share, width), BF16),
             pltpu.VMEM((nx * share, hidden), BF16),
-            pltpu.VMEM((nz, nx, share, width), BF16),
-            pltpu.VMEM((nz, nx, share, width), BF16),
-            pltpu.VMEM((nz, share, width), BF16),
-            pltpu.VMEM((nz, share, width), BF16),
+            pltpu.VMEM((nz, nx, SLICES, share, strip), BF16),
+            pltpu.VMEM((nz, nx, SLICES, share, strip), BF16),
+            pltpu.VMEM((nz, SLICES, share, strip), BF16),
+            pltpu.VMEM((nz, SLICES, share, strip), BF16),
             pltpu.VMEM((n_tp, share, feats), BF16),
             pltpu.VMEM((n_tp, share, feats), BF16),
             dma((8 + heads,)),
-            dma((heads,)),
             dma((2 * ny,)),
             dma((n_tp,)),
             dma((CHUNKS, ny)),
@@ -351,19 +361,19 @@
             dma((CHUNKS, nz)),
             dma((CHUNKS, nz, nx)),
             dma((nz, nx, CHUNKS)),
-            dma((nz, nx)),
-            dma((nz, nx)),
-            dma((nz,)),
-            dma((nz,)),
+            dma((nz, nx, SLICES)),
+            dma((nz, nx, SLICES)),
+            dma((nz, SLICES)),
+            dma((nz, SLICES)),
             dma((n_tp,)),
             dma((n_tp,)),
         ],
         compiler_params=pltpu.CompilerParams(
-            collective_id=0, has_side_effects=True, vmem_limit_bytes=56 * 1024 * 1024
+            collective_id=0, has_side_effects=True, vmem_limit_bytes=48 * 1024 * 1024
         ),
     )(
-        tokens, jnp.transpose(states, (1, 2, 3, 0)), mix_gain[None], w_query, w_key, w_value,
-        w_gate, head_gain[None], w_output, channel_gain[None], w_up, w_down, turn,
+        tokens, jnp.transpose(states, (1, 2, 3, 0)), mix_gain, w_query, w_key, w_value,
+        w_gate, head_gain, w_output, channel_gain, w_up, w_down, turn,
     )
     return (layer_out, jnp.transpose(new_states, (3, 0, 1, 2)))
 

time: 76.4 us -> 62.1 us (0.81)
  local copies, waits for them, and re-layouts: 13.8 us -> 4.05 us
  Pallas kernels: 61.6 us -> 57.2 us
    unnamed x2, local copies, waits for them, and re-layouts: 10 us -> 4.05 us
    pallas_call x1, Pallas kernels: 61.6 us -> 57.2 us  [local(): pl.pallas_call(functools.partial(kernel, sizes), out_shape=(pltpu.VMEM((r...]
    broadcast_in_dim x3 -> x0, local copies, waits for them, and re-layouts: 3.81 us -> none  [the longest x1 1.29 us: local(): mix_gain[None]]
where the time goes in v2:
time: 62.1 us; the launch traced here: 61.9 us
  Pallas kernels  57.2 us (92%)
  local copies, waits for them, and re-layouts  4.05 us (7%)
  between operations  0.64 us (1%)
    pallas_call x1, Pallas kernels, local(): pl.pallas_call(functools.partial(kernel, sizes), out_shape=(pltpu.VMEM((r...  57.2 us
    unnamed x2, local copies, waits for them, and re-layouts  4.05 us

profile of v2, /device:TPU:0, one launch (start us, length us, event | category | flops | bytes accessed | tf_op | source)
XLA Modules:
  0.0 61.9 jit_solution(10215700134166286542)
XLA Ops:
  0.6 57.2 %shard_map.140 = (bf16[128,512]{1,0:T(8,128)(2,1)S(1)}, f32[4,64,64,128]{3,2,1,0:T(8,128)S(1)}) custom-call(bf16[128,512]{1,0:T(8,128)(2,1)} %tok_hbm.1, f32[4,64,64,128]{3,2,1,0:T(8,128)} %bitcast.3, bf16[2048]{0:T(1024)(128)(2,1)} %mix_gain.1, bf16[2048,256]{1,0:T(8,128)(2,1)} %wq_hbm.1, bf16[2048,256]{1,0:T(8,128)(2,1)} %wk_hbm.1, ...), custom_call_target="tpu_custom_call" | custom-call | tf_op jit(solution)/shard_map/pallas_call | solution.py:320
  57.9 0.7 %copy.17 = bf16[128,512]{1,0:T(8,128)(2,1)} copy(bf16[128,512]{1,0:T(8,128)(2,1)S(1)} %get-tuple-element.6) | data formatting | bytes 262144
  58.5 3.4 %copy.18 = f32[128,4,64,64]{0,3,2,1:T(8,128)} copy(f32[128,4,64,64]{0,3,2,1:T(8,128)S(1)} %bitcast.2) | data formatting | bytes 16777216
